TPU v7x, 32 devices: a whole 2x2x4 slice. The times are simulated.
32 devices in a mesh: gr: 2 (over x), sp: 8 (over z, y), tp: 2 (over core).
Axes of the slice: x: 2, y: 2, z: 4, core: 2. Of those that a mesh axis runs over, the one named last changes fastest.
Arguments:
- inputs: bfloat16 [4096, 2048], P(('gr', 'sp'), 'tp'), parts along dimension 0, may hold values from -6 to 6
- x_weight: bfloat16 [2048, 4096], P(None, 'tp'), may hold values from -0.125 to 0.125
- b_weight: bfloat16 [2048, 2048], P(None, 'tp'), may hold values from -0.125 to 0.125
- dt_weight: bfloat16 [2048, 128], replicated, may hold values from -0.125 to 0.125
- dt_bias: float32 [2, 64], replicated, may hold values from -2 to -1
- decay_rate: float32 [2, 64], replicated, may hold values from 0.3 to 10
- conv_x: bfloat16 [5, 4096], P(None, 'tp'), may hold values from -2.5 to 2.5
- conv_b: bfloat16 [5, 2048], P(None, 'tp'), may hold values from -2.5 to 2.5
- query_c: bfloat16 [2, 16, 128], P('gr', 'tp'), parts along dimension 0, may hold values from -6 to 6
- query_gate: bfloat16 [2, 64, 64], P('gr', 'tp'), parts along dimension 0, may hold values from -6 to 6
- read_span: int32 [2], P('gr'), parts along dimension 0, may hold values from 0 to 15
- read_gain: float32 [64, 64], P('tp'), may hold values from 0.1 to 1.9
Outputs:
- span_cache: bfloat16 [32, 2, 64, 8192], P('gr', None, 'tp', 'sp'), parts along dimension 0
- first_read: bfloat16 [2, 64, 64], P('gr', 'tp'), parts along dimension 0
There are 2 independent parts, one for each index of `gr`. A program takes and returns all parts, laid end to end along the dimension named above; an argument that names none is the same for every part. Nothing has to cross between parts.
Inputs may be any that keep to these rules, and one draw needn't show every extreme that they name: read_span holds one span index from 0 to 15.
All inputs are finite; a program needn't handle non-finite values.
Results may differ from a plain program's by a relative error of at most 0.009.
Values may be sent and summed in bfloat16 or wider, within the bound.
A program may use at most 64 MiB of HBM per device.

v0:
```python
import jax
import jax.numpy as jnp
from jax import lax
from jax.sharding import PartitionSpec as P

H = 64
P_SIZE = 64
G = 16
N = 128
KW = 5
SPAN = 128
EPSILON = 1e-06


def extended(shard, sides, width):
    for axis, dim in sides:
        size, length = (lax.axis_size(axis), shard.shape[dim])
        up = [(i, (i + 1) % size) for i in range(size - 1)]
        down = [(j, i) for i, j in up]
        last = lax.slice_in_dim(shard, length - width, length, axis=dim)
        initial = lax.slice_in_dim(shard, 0, width, axis=dim)
        before = lax.ppermute(last, axis, up)
        after = lax.ppermute(initial, axis, down)
        shard = jnp.concatenate([before, shard, after], axis=dim)
    return shard


def span_states(value_rows, key_rows, step_sizes, log_decay):
    running = jnp.cumsum(log_decay, axis=1)
    closing = running[:, -1]
    forward = jnp.exp(closing[:, None, 0] - running[:, :, 0]) * step_sizes[:, :, 0]
    backward = jnp.exp(running[:, :, 1] - log_decay[:, :, 1]) * step_sizes[:, :, 1]
    weights = jnp.stack([forward, backward], axis=2)
    states = jnp.einsum(
        "kseh,kshn,kshp->kehnp",
        weights,
        key_rows.astype(jnp.float32),
        value_rows.astype(jnp.float32),
    )
    return (states, closing)


def read_weights(span_logs, chosen):
    span_count = span_logs.shape[0]
    ahead_sum = jnp.cumsum(span_logs[:, 0], axis=0)
    behind = jnp.flip(jnp.cumsum(jnp.flip(span_logs[:, 1], 0), axis=0), 0)
    positions = jnp.arange(span_count, dtype=jnp.int32)[:, None]
    ahead_pick = lax.dynamic_slice_in_dim(ahead_sum, chosen, 1, 0)
    behind_pick = lax.dynamic_slice_in_dim(behind, chosen, 1, 0)
    before = positions <= chosen
    after = positions >= chosen
    forward = jnp.where(before, jnp.exp(jnp.where(before, ahead_pick - ahead_sum, 0.0)), 0.0)
    backward = jnp.where(after, jnp.exp(jnp.where(after, behind_pick - behind, 0.0)), 0.0)
    return jnp.stack([forward, backward], axis=1)


def per_device(
    inputs,
    x_weight,
    b_weight,
    dt_weight,
    dt_bias,
    decay_rate,
    conv_x,
    conv_b,
    query_c,
    query_gate,
    read_span,
    read_gain,
):
    tokens = inputs.shape[0]
    heads_local = x_weight.shape[1] // P_SIZE
    per_group = H // G
    tp_index = lax.axis_index("tp")
    sp_index = lax.axis_index("sp")
    dt_local = lax.dynamic_slice_in_dim(
        dt_weight.reshape(dt_weight.shape[0], 2, H), tp_index * heads_local, heads_local, 2
    )
    dt_local = dt_local.reshape(dt_weight.shape[0], 2 * heads_local)
    slab_piece = lax.all_gather(inputs, "tp", axis=1, tiled=True)
    x_part = jnp.dot(slab_piece, x_weight, preferred_element_type=jnp.float32)
    b_part = jnp.dot(slab_piece, b_weight, preferred_element_type=jnp.float32)
    dt_part = jnp.dot(slab_piece, dt_local, preferred_element_type=jnp.float32)
    joined = jnp.concatenate([x_part.astype(jnp.bfloat16), b_part.astype(jnp.bfloat16)], axis=1)
    reach = KW // 2
    padded = extended(joined, (("sp", 0),), reach)
    taps = jnp.concatenate([conv_x, conv_b], axis=1)
    mixed_rows = jnp.zeros(joined.shape, jnp.float32)
    for offset in range(KW):
        mixed_rows = mixed_rows + taps[offset].astype(jnp.float32) * padded[
            offset : offset + tokens
        ].astype(jnp.float32)
    mixed_rows = jax.nn.silu(mixed_rows).astype(jnp.bfloat16)
    split_at = x_weight.shape[1]
    values = mixed_rows[:, :split_at]
    key_rows = mixed_rows[:, split_at:]
    length = tokens * lax.axis_size("sp")
    bias_local = lax.dynamic_slice_in_dim(dt_bias, tp_index * heads_local, heads_local, 1)
    rate_local = lax.dynamic_slice_in_dim(decay_rate, tp_index * heads_local, heads_local, 1)
    dt_raw = dt_part.astype(jnp.bfloat16).reshape(tokens, 2, heads_local)
    step_sizes = jax.nn.softplus(dt_raw.astype(jnp.float32) + bias_local)
    log_decay = -(step_sizes * rate_local) / length
    span_count = tokens // SPAN
    value_rows = values.reshape(span_count, SPAN, heads_local, P_SIZE)
    group_keys = key_rows.reshape(span_count, SPAN, heads_local // per_group, N)
    group_keys = jnp.repeat(group_keys, per_group, axis=2)
    states, closing = span_states(
        value_rows,
        group_keys,
        step_sizes.reshape(span_count, SPAN, 2, heads_local),
        log_decay.reshape(span_count, SPAN, 2, heads_local),
    )
    local_rows = states.reshape(span_count, 2, heads_local, N * P_SIZE).astype(jnp.bfloat16)
    all_logs = lax.all_gather(closing, "sp", axis=0, tiled=True)
    weights = read_weights(all_logs, read_span[0])
    cache_rows = lax.all_to_all(local_rows, "sp", split_axis=3, concat_axis=0, tiled=True)
    columns = cache_rows.shape[3] // P_SIZE
    gathered = jnp.einsum("jeh,jehx->hx", weights, cache_rows.astype(jnp.float32)).reshape(
        heads_local, columns, P_SIZE
    )
    picked = lax.dynamic_slice_in_dim(query_c[0], sp_index * columns, columns, 1)
    query_cols = jnp.repeat(picked.astype(jnp.float32), per_group, axis=0)
    partial_read = jnp.einsum("hnp,hn->hp", gathered, query_cols)
    read_total = lax.psum(partial_read, "sp")
    gated_read = read_total * jax.nn.silu(query_gate[0].astype(jnp.float32))
    square_sum = lax.psum(jnp.sum(gated_read * gated_read), "tp")
    mean_square = square_sum / (H * P_SIZE)
    first_read = (gated_read * lax.rsqrt(mean_square + EPSILON) * read_gain)[None].astype(
        jnp.bfloat16
    )
    return (cache_rows, first_read)


def solution(mesh):
    return jax.shard_map(
        per_device,
        mesh=mesh,
        in_specs=(
            P(("gr", "sp"), "tp"),
            P(None, "tp"),
            P(None, "tp"),
            P(),
            P(),
            P(),
            P(None, "tp"),
            P(None, "tp"),
            P("gr", "tp", None),
            P("gr", "tp", None),
            P("gr"),
            P("tp", None),
        ),
        out_specs=(P("gr", None, "tp", "sp"), P("gr", "tp", None)),
        check_vma=False,
    )
```

profile of v0, /device:TPU:0, one launch (start us, length us, event | category | flops | bytes accessed | tf_op | source)
XLA Modules:
  0.0 222.9 jit_solution(17773302501208012883)
XLA Ops:
  7.2 0.0 all-gather.3.cloned.1.call-start
  7.2 0.7 all-gather.3.cloned.1.call-update
  7.9 0.8 constant_dynamic-update-slice_fusion.1
  8.7 0.8 constant_dynamic-slice_fusion.2
  9.4 1.2 copy.63
  10.7 0.7 constant_dynamic-update-slice_fusion
  11.5 9.8 %all-gather.3.cloned.1.call-done = bf16[256,2048]{1,0:T(8,128)(2,1)} async-done(((bf16[256,1024]{1,0:T(8,128)(2,1)}), bf16[256,2048]{1,0:T(8,128)(2,1)}) %all-gather.3.cloned.1.call-update) | async-done | bytes 1048592 | tf_op jit(solution)/shard_map/all_gather | solution.py:80
  21.3 0.0 copy-start.1
  21.3 1.8 fusion.9
  23.1 0.1 negate_multiply_fusion
  23.2 0.2 copy.65
  23.4 0.1 fusion.26
  23.5 0.2 fusion.24
  23.7 0.1 copy.86
  23.8 0.1 copy.87
  23.9 0.0 copy-done.1
  23.9 0.0 copy-start.5
  23.9 5.9 %convolution_convert_fusion = bf16[256,2048]{1,0:T(8,128)(2,1)S(1)} fusion(bf16[256,2048]{1,0:T(8,128)(2,1)S(1)} %copy-done.1, bf16[2048,2048]{1,0:T(8,128)(2,1)} %param.13), kind=kOutput, calls=%fused_computation.3 | convolution fusion | flops 2148007936 | bytes 10485760 | tf_op jit(solution)/shard_map/dot_general | solution.py:81
  29.8 0.0 copy-done.5
  29.8 1.3 convolution_convert_fusion.1
  31.1 3.6 %collective-permute-start = (bf16[2,3072]{1,0:T(2,128)(2,1)S(1)}, bf16[2,3072]{1,0:T(2,128)(2,1)S(1)}, u32[]{:S(2)}, u32[]{:S(2)}) collective-permute-start(bf16[2,3072]{1,0:T(2,128)(2,1)S(1)} %get-tuple-element.6), channel_id=1, source_target_pairs={{0,2},{2,4},{4,6},{6,8},{8,10},{10,12},{12,14},{1,3},{3,5},{5,7},{... | collective-permute-start | bytes 36872 | tf_op jit(solution)/shard_map/ppermute | solution.py:22
  34.8 1.3 collective-permute-start.1
  36.1 0.1 slice_multiply_fusion.1
  36.2 0.1 copy.68
  36.2 0.0 collective-permute-done
  36.3 4.1 %collective-permute-done.1 = bf16[2,3072]{1,0:T(2,128)(2,1)S(1)} collective-permute-done((bf16[2,3072]{1,0:T(2,128)(2,1)S(1)}, bf16[2,3072]{1,0:T(2,128)(2,1)S(1)}, u32[]{:S(2)}, u32[]{:S(2)}) %collective-permute-start.1) | collective-permute-done | bytes 12320 | tf_op jit(solution)/shard_map/ppermute | solution.py:23
  40.4 0.5 maximum_maximum_fusion
  40.9 2.9 %multiply_convert_fusion = bf16[256,3072]{1,0:T(8,128)(2,1)S(1)} fusion(bf16[256,1024]{1,0:T(8,128)(2,1)S(1)} %convolution_convert_fusion.1, bf16[256,2048]{1,0:T(8,128)(2,1)S(1)} %convolution_convert_fusion, bf16[258,3072]{1,0:T(8,128)(2,1)S(1)} %get-tuple-element.5, bf16[258,3072]{1,0:T(8,128)(2,1)S(1)} %get-tuple-element.4, f32[3072]{0:T(1024)S(1)} %bitcast.103, ...), kind=kLoop, calls=%fused_computation.2 | loop fusion | flops 17301504 | bytes 9498624 | tf_op jit(solution)/shard_map/convert_element_type | solution.py:93
  43.7 0.2 slice_convert_fusion
  44.0 3.0 %reshape.152 = f32[2,128,32,64]{3,2,1,0:T(8,128)} reshape(f32[256,2048]{1,0:T(8,128)S(1)} %slice_convert_fusion) | data formatting | bytes 4194304 | tf_op jit(solution)/shard_map/convert.7
  47.0 3.8 %copy.62 = f32[2,128,32,64]{1,3,2,0:T(8,128)S(1)} copy(f32[2,128,32,64]{3,2,1,0:T(8,128)} %reshape.152) | data formatting | bytes 4194304 | tf_op jit(solution)/shard_map/convert.7
  50.8 0.1 copy.88
  50.9 0.1 copy.69
  51.0 0.6 broadcast_in_dim.43
  51.6 2.0 convert_bitcast_fusion
  53.6 14.1 %copy.82 = bf16[2,2,32,128,64]{2,1,0,4,3:T(2,128)(2,1)} copy(bf16[2,2,32,128,64]{3,4,1,2,0:T(8,128)(2,1)} %convert_bitcast_fusion) | data formatting | bytes 4194304 | tf_op jit(solution)/shard_map/convert_element_type | solution.py:113
  67.7 11.2 %reshape.153 = bf16[8,2,65536]{2,1,0:T(2,128)(2,1)} reshape(bf16[8192,2,2,32]{3,2,1,0:T(2,128)(2,1)} %bitcast.92) | data formatting | bytes 4194304
  78.8 0.0 copy-start.4
  78.9 5.6 %all-to-all-start = ((bf16[8,2,65536]{2,1,0:T(2,128)(2,1)}), bf16[8,2,65536]{2,1,0:T(2,128)(2,1)S(1)}, u32[]{:S(2)}, u32[]{:S(2)}) async-start(bf16[8,2,65536]{2,1,0:T(2,128)(2,1)} %reshape.153), calls=%async_computation | async-start | bytes 4194304 | tf_op jit(solution)/shard_map/all_to_all | solution.py:116
  85.1 0.0 copy-done.4
  85.2 0.1 bitcast_convert_fusion
  85.2 65.2 %all-gather = f32[16,1,2,32]{3,2,1,0:T(2,128)S(1)} all-gather(f32[2,1,2,32]{3,2,1,0:T(2,128)S(1)} %get-tuple-element.8), channel_id=2, replica_groups=mesh['gr'=2,'sp'=8,'tp'=2] {'sp'}, dimensions={0}, use_global_device_ids=true | all-gather | bytes 4608 | tf_op jit(solution)/shard_map/all_gather | solution.py:114
  150.5 0.1 select_bitcast_fusion
  150.6 0.1 fusion.20
  150.7 0.1 copy.75
  150.8 0.0 all-to-all-done
  150.8 6.6 %reshape.154 = bf16[8192,2,2,32]{3,2,1,0:T(2,128)(2,1)} reshape(bf16[8,2,65536]{2,1,0:T(2,128)(2,1)S(1)} %all-to-all-done) | data formatting | bytes 4194304
  157.4 0.0 copy-start.2
  157.4 17.8 %copy.84 = bf16[2,2,32,8,1024]{4,2,1,0,3:T(8,128)(2,1)S(1)} copy(bf16[2,2,32,8,1024]{2,1,0,4,3:T(2,128)(2,1)} %bitcast.93) | data formatting | bytes 4194304 | tf_op jit(solution)/shard_map/all_to_all | solution.py:116
  175.2 0.0 copy-start
  175.2 0.0 copy-start.3
  175.2 2.4 %fusion.2 = bf16[32,1,1024,1]{2,1,3,0:T(2,128)(2,1)S(1)} fusion(bf16[16,2,32,1]{0,3,1,2:T(2,128)(2,1)S(1)} %copy.75, bf16[16,2,32,1024]{3,2,1,0:T(8,128)(2,1)S(1)} %bitcast.95), kind=kOutput, calls=%fused_computation.7 | convolution fusion | flops 2097152 | bytes 2164736 | tf_op jit(solution)/shard_map/jeh,jehx->hx/dot_general | solution.py:118
  177.6 0.1 reshape.135
  177.8 0.2 fusion.27
  178.0 33.1 %psum.14 = f32[32,64]{1,0:T(8,128)S(1)} all-reduce(f32[32,64]{1,0:T(8,128)S(1)} %bitcast.110), channel_id=1, replica_groups=mesh['gr'=2,'sp'=8,'tp'=2] {'sp'}, use_global_device_ids=true, to_apply=%region_3.4 | all-reduce | flops 2048 | bytes 16384 | tf_op jit(solution)/shard_map/psum | solution.py:124
  211.0 0.0 copy-done.2
  211.0 0.6 multiply_reduce_fusion
  211.7 3.1 %psum.15 = f32[]{:T(128)} all-reduce(f32[]{:T(128)} %multiply_reduce_fusion), channel_id=1, replica_groups=mesh['gr'=2,'sp'=8,'tp'=2] {'tp'}, use_global_device_ids=true, to_apply=%region_5.6 | all-reduce | flops 1 | bytes 8 | tf_op jit(solution)/shard_map/psum | solution.py:126
  215.4 0.0 copy-done.3
  215.4 0.6 fusion.17
  216.1 0.0 copy-done
  (19 shorter events, 0.3 us)
Async XLA Ops:
  7.2 14.1 %all-gather.3.cloned.1.call-start = ((), (), s32[]{:S(2)}) async-start(), calls=%async_computation.1 | async-start | bytes 1572864 | tf_op jit(solution)/shard_map/all_gather | solution.py:80
  21.3 2.6 %copy-start.1 = (bf16[256,2048]{1,0:T(8,128)(2,1)S(1)}, bf16[256,2048]{1,0:T(8,128)(2,1)}, u32[]{:S(2)}) copy-start(bf16[256,2048]{1,0:T(8,128)(2,1)} %all-gather.3.cloned.1.call-done) | copy-start | bytes 3145732
  23.9 5.9 %copy-start.5 = (bf16[2048,1024]{1,0:T(8,128)(2,1)S(1)}, bf16[2048,1024]{1,0:T(8,128)(2,1)}, u32[]{:S(2)}) copy-start(bf16[2048,1024]{1,0:T(8,128)(2,1)} %param.14) | copy-start | bytes 12582916
  31.1 5.1 %collective-permute-start = (bf16[2,3072]{1,0:T(2,128)(2,1)S(1)}, bf16[2,3072]{1,0:T(2,128)(2,1)S(1)}, u32[]{:S(2)}, u32[]{:S(2)}) collective-permute-start(bf16[2,3072]{1,0:T(2,128)(2,1)S(1)} %get-tuple-element.6), channel_id=1, source_target_pairs={{0,2},{2,4},{4,6},{6,8},{8,10},{10,12},{12,14},{1,3},{3,5},{5,7},{... | collective-permute-start | bytes 36872 | tf_op jit(solution)/shard_map/ppermute | solution.py:22
  34.8 5.6 %collective-permute-start.1 = (bf16[2,3072]{1,0:T(2,128)(2,1)S(1)}, bf16[2,3072]{1,0:T(2,128)(2,1)S(1)}, u32[]{:S(2)}, u32[]{:S(2)}) collective-permute-start(bf16[2,3072]{1,0:T(2,128)(2,1)S(1)} %get-tuple-element.7), channel_id=1, source_target_pairs={{2,0},{4,2},{6,4},{8,6},{10,8},{12,10},{14,12},{3,1},{5,3},{7,5},{... | collective-permute-start | bytes 36872 | tf_op jit(solution)/shard_map/ppermute | solution.py:23
  78.8 6.3 %copy-start.4 = (bf16[1,8,128]{2,1,0:T(8,128)(2,1)S(1)}, bf16[1,8,128]{2,1,0:T(8,128)(2,1)}, u32[]{:S(2)}) copy-start(bf16[1,8,128]{2,1,0:T(8,128)(2,1)} %param.20) | copy-start | bytes 6148
  78.9 72.0 %all-to-all-start = ((bf16[8,2,65536]{2,1,0:T(2,128)(2,1)}), bf16[8,2,65536]{2,1,0:T(2,128)(2,1)S(1)}, u32[]{:S(2)}, u32[]{:S(2)}) async-start(bf16[8,2,65536]{2,1,0:T(2,128)(2,1)} %reshape.153), calls=%async_computation | async-start | bytes 4194304 | tf_op jit(solution)/shard_map/all_to_all | solution.py:116
  157.4 53.7 %copy-start.2 = (bf16[1,32,64]{2,1,0:T(8,128)(2,1)S(1)}, bf16[1,32,64]{2,1,0:T(8,128)(2,1)}, u32[]{:S(2)}) copy-start(bf16[1,32,64]{2,1,0:T(8,128)(2,1)} %param.21) | copy-start | bytes 12292
  175.2 40.9 %copy-start = (bf16[2,2,32,8,1024]{4,2,1,0,3:T(8,128)(2,1)}, bf16[2,2,32,8,1024]{4,2,1,0,3:T(8,128)(2,1)S(1)}, u32[]{:S(2)}) copy-start(bf16[2,2,32,8,1024]{4,2,1,0,3:T(8,128)(2,1)S(1)} %copy.84) | copy-start | bytes 6291460
  175.2 40.2 %copy-start.3 = (f32[32,64]{1,0:T(8,128)S(1)}, f32[32,64]{1,0:T(8,128)}, u32[]{:S(2)}) copy-start(f32[32,64]{1,0:T(8,128)} %param.23) | copy-start | bytes 24580
Sparse Core Ops, SparseCore 0:
  9.5 11.7 all-gather.2
where the time goes:
time: 224 us; the launch traced here: 223 us
  blocking collectives  101 us (45%)
  local copies, waits for them, and re-layouts  61.6 us (28%)
  between operations  15.7 us (7%)
  waiting for transfers between devices  14.6 us (7%)
  matrix products  13.5 us (6%)
  starting transfers between devices  10.6 us (5%)
  other arithmetic  5.54 us (2%)
    all_gather x1, blocking collectives, per_device(): all_logs = lax.all_gather(closing, 'sp', axis=0, tiled=True)  65.2 us
    psum x1, blocking collectives, per_device(): read_total = lax.psum(partial_read, 'sp')  33.1 us
    unnamed x20, local copies, waits for them, and re-layouts  20.1 us
    all_to_all x1, local copies, waits for them, and re-layouts, per_device(): lax.all_to_all(local_rows, 'sp', split_axis=3, concat_axis=0, tiled=True)  17.8 us
    convert_element_type x1, local copies, waits for them, and re-layouts, per_device(): states.reshape(span_count, 2, heads_local, N * P_SIZE).astype(jnp.bfloat16)  14.1 us
    all_gather x1, waiting for transfers between devices, per_device(): slab_piece = lax.all_gather(inputs, 'tp', axis=1, tiled=True)  9.82 us
    another operation x2, local copies, waits for them, and re-layouts  6.77 us
    dot_general x1, matrix products, per_device(): x_part = jnp.dot(slab_piece, x_weight, preferred_element_type=jnp.float32)  5.86 us
  transfers between devices with their start and end apart: 4, of which 2 were waited for; matrix products, arithmetic and copies ran while one was open for 2% of the time, Pallas kernels for 0%

commit v1 on v0

--- a/solution.py
+++ b/solution.py
@@ -2,6 +2,7 @@
 import jax.numpy as jnp
 from jax import lax
 from jax.sharding import PartitionSpec as P
+from jax.lax import all_to_all, axis_size
 
 H = 64
 P_SIZE = 64
@@ -10,6 +11,13 @@
 KW = 5
 SPAN = 128
 EPSILON = 1e-06
+
+
+def fit_the_pieces_all(message):
+    r1 = jnp.stack(jnp.split(message, axis_size("sp"), 3), 0)
+    field_out = all_to_all(r1, "sp", split_axis=0, concat_axis=0)
+    response = jnp.concatenate(field_out, 0)
+    return response
 
 
 def extended(shard, sides, width):
@@ -113,7 +121,7 @@
     local_rows = states.reshape(span_count, 2, heads_local, N * P_SIZE).astype(jnp.bfloat16)
     all_logs = lax.all_gather(closing, "sp", axis=0, tiled=True)
     weights = read_weights(all_logs, read_span[0])
-    cache_rows = lax.all_to_all(local_rows, "sp", split_axis=3, concat_axis=0, tiled=True)
+    cache_rows = fit_the_pieces_all(local_rows)
     columns = cache_rows.shape[3] // P_SIZE
     gathered = jnp.einsum("jeh,jehx->hx", weights, cache_rows.astype(jnp.float32)).reshape(
         heads_local, columns, P_SIZE

time: 224 us -> 192 us (0.86)
  local copies, waits for them, and re-layouts: 61.6 us -> 29.5 us
    all_to_all x1 -> x0, local copies, waits for them, and re-layouts: 17.8 us -> none  [per_device(): lax.all_to_all(local_rows, 'sp', split_axis=3, concat_axis=0, tiled=True)]
    unnamed x20 -> x24, local copies, waits for them, and re-layouts: 20.1 us -> 8.68 us
    convert_element_type x1 -> x2, local copies, waits for them, and re-layouts: 14.1 us -> 10.4 us  [per_device(): states.reshape(span_count, 2, heads_local, N * P_SIZE).astype(jnp.bfloat16)]
    another operation x2 -> x3, local copies, waits for them, and re-layouts: 6.77 us -> 7.5 us
where the time goes in v1:
time: 192 us; the launch traced here: 191 us
  blocking collectives  101 us (53%)
  local copies, waits for them, and re-layouts  29.5 us (15%)
  between operations  15.7 us (8%)
  waiting for transfers between devices  14.6 us (8%)
  matrix products  13.5 us (7%)
  starting transfers between devices  10.6 us (6%)
  other arithmetic  5.54 us (3%)
    all_gather x1, blocking collectives, per_device(): all_logs = lax.all_gather(closing, 'sp', axis=0, tiled=True)  65.1 us
    psum x1, blocking collectives, per_device(): read_total = lax.psum(partial_read, 'sp')  33.1 us
    convert_element_type x2, local copies, waits for them, and re-layouts, per_device(): states.reshape(span_count, 2, heads_local, N * P_SIZE).astype(jnp.bfloat16)  10.4 us
    all_gather x1, waiting for transfers between devices, per_device(): slab_piece = lax.all_gather(inputs, 'tp', axis=1, tiled=True)  9.82 us
    unnamed x24, local copies, waits for them, and re-layouts  8.68 us
    another operation x2, local copies, waits for them, and re-layouts  6.78 us
    dot_general x1, matrix products, per_device(): x_part = jnp.dot(slab_piece, x_weight, preferred_element_type=jnp.float32)  5.86 us
    all_to_all x1, starting transfers between devices, fit_the_pieces_all(): field_out = all_to_all(r1, 'sp', split_axis=0, concat_axis=0)  5.63 us
  transfers between devices with their start and end apart: 4, of which 2 were waited for; matrix products, arithmetic and copies ran while one was open for 2% of the time, Pallas kernels for 0%

profile of v1, /device:TPU:0, one launch (start us, length us, event | category | flops | bytes accessed | tf_op | source)
XLA Modules:
  0.0 190.8 jit_solution(12353510731553552230)
XLA Ops:
  7.2 0.0 all-gather.3.cloned.1.call-start
  7.2 0.7 all-gather.3.cloned.1.call-update
  7.9 0.8 constant_dynamic-update-slice_fusion.1
  8.7 0.8 constant_dynamic-slice_fusion.2
  9.4 1.2 copy.49
  10.7 0.7 constant_dynamic-update-slice_fusion
  11.5 9.8 %all-gather.3.cloned.1.call-done = bf16[256,2048]{1,0:T(8,128)(2,1)} async-done(((bf16[256,1024]{1,0:T(8,128)(2,1)}), bf16[256,2048]{1,0:T(8,128)(2,1)}) %all-gather.3.cloned.1.call-update) | async-done | bytes 1048592 | tf_op jit(solution)/shard_map/all_gather | solution.py:88
  21.3 0.0 copy-start
  21.3 1.8 fusion.9
  23.1 0.1 negate_multiply_fusion
  23.2 0.2 copy.51
  23.4 0.1 fusion.34
  23.5 0.2 fusion.32
  23.7 0.1 copy.65
  23.8 0.1 copy.66
  23.9 0.0 copy-done
  23.9 0.0 copy-start.4
  23.9 5.9 %convolution_convert_fusion = bf16[256,2048]{1,0:T(8,128)(2,1)S(1)} fusion(bf16[256,2048]{1,0:T(8,128)(2,1)S(1)} %copy-done, bf16[2048,2048]{1,0:T(8,128)(2,1)} %param.13), kind=kOutput, calls=%fused_computation.3 | convolution fusion | flops 2148007936 | bytes 10485760 | tf_op jit(solution)/shard_map/dot_general | solution.py:89
  29.8 0.0 copy-done.4
  29.8 1.3 convolution_convert_fusion.1
  31.1 3.6 %collective-permute-start = (bf16[2,3072]{1,0:T(2,128)(2,1)S(1)}, bf16[2,3072]{1,0:T(2,128)(2,1)S(1)}, u32[]{:S(2)}, u32[]{:S(2)}) collective-permute-start(bf16[2,3072]{1,0:T(2,128)(2,1)S(1)} %get-tuple-element.6), channel_id=1, source_target_pairs={{0,2},{2,4},{4,6},{6,8},{8,10},{10,12},{12,14},{1,3},{3,5},{5,7},{... | collective-permute-start | bytes 36872 | tf_op jit(solution)/shard_map/ppermute | solution.py:30
  34.8 1.3 collective-permute-start.1
  36.1 0.1 slice_multiply_fusion.1
  36.2 0.1 copy.54
  36.2 0.0 collective-permute-done
  36.3 4.1 %collective-permute-done.1 = bf16[2,3072]{1,0:T(2,128)(2,1)S(1)} collective-permute-done((bf16[2,3072]{1,0:T(2,128)(2,1)S(1)}, bf16[2,3072]{1,0:T(2,128)(2,1)S(1)}, u32[]{:S(2)}, u32[]{:S(2)}) %collective-permute-start.1) | collective-permute-done | bytes 12320 | tf_op jit(solution)/shard_map/ppermute | solution.py:31
  40.4 0.5 maximum_maximum_fusion
  40.9 2.9 %multiply_convert_fusion = bf16[256,3072]{1,0:T(8,128)(2,1)S(1)} fusion(bf16[256,1024]{1,0:T(8,128)(2,1)S(1)} %convolution_convert_fusion.1, bf16[256,2048]{1,0:T(8,128)(2,1)S(1)} %convolution_convert_fusion, bf16[258,3072]{1,0:T(8,128)(2,1)S(1)} %get-tuple-element.5, bf16[258,3072]{1,0:T(8,128)(2,1)S(1)} %get-tuple-element.4, f32[3072]{0:T(1024)S(1)} %bitcast.128, ...), kind=kLoop, calls=%fused_computation.2 | loop fusion | flops 17301504 | bytes 9498624 | tf_op jit(solution)/shard_map/convert_element_type | solution.py:101
  43.7 0.2 slice_convert_fusion
  44.0 3.0 %reshape.156 = f32[2,128,32,64]{3,2,1,0:T(8,128)} reshape(f32[256,2048]{1,0:T(8,128)S(1)} %slice_convert_fusion) | data formatting | bytes 4194304 | tf_op jit(solution)/shard_map/convert.7
  47.0 3.8 %copy.48 = f32[2,128,32,64]{1,3,2,0:T(8,128)S(1)} copy(f32[2,128,32,64]{3,2,1,0:T(8,128)} %reshape.156) | data formatting | bytes 4194304 | tf_op jit(solution)/shard_map/convert.7
  50.8 0.1 copy.67
  50.9 0.1 copy.55
  51.0 0.6 broadcast_in_dim.43
  51.6 2.0 %convert_bitcast_fusion = bf16[2,2,32,128,64]{3,4,1,2,0:T(8,128)(2,1)} fusion(bf16[2,128,32,128,1]{3,1,4,2,0:T(8,128)(2,1)S(1)} %bitcast.119, f32[2,128,32,2]{1,3,2,0:T(2,128)S(1)} %copy.54, f32[2,128,32,64]{1,3,2,0:T(8,128)S(1)} %copy.48), kind=kOutput, calls=%fused_computation.9 | convolution fusion | flops 270532608 | bytes 6356992 | tf_op jit(solution)/shard_map/kseh,kshn,kshp->kehnp/dot_general | solution.py:42
  53.6 4.8 %copy.56 = bf16[2,2,32,128,64]{4,3,2,1,0:T(8,128)(2,1)} copy(bf16[2,2,32,128,64]{3,4,1,2,0:T(8,128)(2,1)} %convert_bitcast_fusion) | data formatting | bytes 4194304 | tf_op jit(solution)/shard_map/convert_element_type | solution.py:121
  58.4 5.7 %convert_element_type.93 = bf16[2,2,32,8192]{3,2,1,0:T(8,128)(2,1)S(1)} reshape(bf16[2,2,32,128,64]{4,3,2,1,0:T(8,128)(2,1)} %copy.56) | data formatting | bytes 4194304 | tf_op jit(solution)/shard_map/convert_element_type | solution.py:121
  64.0 0.7 fusion.17
  64.8 0.7 fusion.16
  65.5 0.7 fusion.15
  66.2 0.7 fusion.14
  66.9 0.7 fusion.13
  67.6 0.7 fusion.12
  68.4 0.7 fusion.11
  69.1 0.7 fusion.10
  69.8 5.6 %all-to-all-start = ((bf16[8,2,2,32,1024]{4,3,2,1,0:T(8,128)(2,1)}), bf16[8,2,2,32,1024]{4,3,2,1,0:T(8,128)(2,1)S(1)}, u32[]{:S(2)}, u32[]{:S(2)}) async-start(bf16[8,2,2,32,1024]{4,3,2,1,0:T(8,128)(2,1)} %fusion.10), calls=%async_computation | async-start | bytes 4194304 | tf_op jit(solution)/shard_map/all_to_all | solution.py:18
  75.5 0.0 copy-start.2
  76.1 0.0 copy-done.3
  76.2 0.1 bitcast_convert_fusion
  76.2 65.1 %all-gather = f32[16,1,2,32]{3,2,1,0:T(2,128)S(1)} all-gather(f32[2,1,2,32]{3,2,1,0:T(2,128)S(1)} %get-tuple-element.8), channel_id=2, replica_groups=mesh['gr'=2,'sp'=8,'tp'=2] {'sp'}, dimensions={0}, use_global_device_ids=true | all-gather | bytes 4608 | tf_op jit(solution)/shard_map/all_gather | solution.py:122
  141.5 0.1 select_bitcast_fusion
  141.6 0.1 fusion.28
  141.7 0.1 copy.58
  141.8 0.0 all-to-all-done
  141.8 2.4 %fusion.2 = bf16[32,1,1024,1]{2,1,3,0:T(2,128)(2,1)S(1)} fusion(bf16[16,2,32,1]{0,3,1,2:T(2,128)(2,1)S(1)} %copy.58, bf16[16,2,32,1024]{3,2,1,0:T(8,128)(2,1)S(1)} %bitcast.120), kind=kOutput, calls=%fused_computation.7 | convolution fusion | flops 2097152 | bytes 2164736 | tf_op jit(solution)/shard_map/jeh,jehx->hx/dot_general | solution.py:126
  144.2 0.1 reshape.139
  144.4 0.2 fusion.35
  144.5 33.1 %psum.14 = f32[32,64]{1,0:T(8,128)S(1)} all-reduce(f32[32,64]{1,0:T(8,128)S(1)} %bitcast.135), channel_id=1, replica_groups=mesh['gr'=2,'sp'=8,'tp'=2] {'sp'}, use_global_device_ids=true, to_apply=%region_3.4 | all-reduce | flops 2048 | bytes 16384 | tf_op jit(solution)/shard_map/psum | solution.py:132
  177.6 0.0 copy-done.1
  177.6 0.6 multiply_reduce_fusion
  178.2 3.1 %psum.15 = f32[]{:T(128)} all-reduce(f32[]{:T(128)} %multiply_reduce_fusion), channel_id=1, replica_groups=mesh['gr'=2,'sp'=8,'tp'=2] {'tp'}, use_global_device_ids=true, to_apply=%region_5.6 | all-reduce | flops 1 | bytes 8 | tf_op jit(solution)/shard_map/psum | solution.py:134
  182.0 0.0 copy-done.2
  182.0 0.6 fusion.25
  182.6 1.3 copy.86
  (21 shorter events, 0.3 us)
Async XLA Ops:
  7.2 14.1 %all-gather.3.cloned.1.call-start = ((), (), s32[]{:S(2)}) async-start(), calls=%async_computation.1 | async-start | bytes 1572864 | tf_op jit(solution)/shard_map/all_gather | solution.py:88
  21.3 2.6 %copy-start = (bf16[256,2048]{1,0:T(8,128)(2,1)S(1)}, bf16[256,2048]{1,0:T(8,128)(2,1)}, u32[]{:S(2)}) copy-start(bf16[256,2048]{1,0:T(8,128)(2,1)} %all-gather.3.cloned.1.call-done) | copy-start | bytes 3145732
  23.9 5.9 %copy-start.4 = (bf16[2048,1024]{1,0:T(8,128)(2,1)S(1)}, bf16[2048,1024]{1,0:T(8,128)(2,1)}, u32[]{:S(2)}) copy-start(bf16[2048,1024]{1,0:T(8,128)(2,1)} %param.14) | copy-start | bytes 12582916
  31.1 5.1 %collective-permute-start = (bf16[2,3072]{1,0:T(2,128)(2,1)S(1)}, bf16[2,3072]{1,0:T(2,128)(2,1)S(1)}, u32[]{:S(2)}, u32[]{:S(2)}) collective-permute-start(bf16[2,3072]{1,0:T(2,128)(2,1)S(1)} %get-tuple-element.6), channel_id=1, source_target_pairs={{0,2},{2,4},{4,6},{6,8},{8,10},{10,12},{12,14},{1,3},{3,5},{5,7},{... | collective-permute-start | bytes 36872 | tf_op jit(solution)/shard_map/ppermute | solution.py:30
  34.8 5.6 %collective-permute-start.1 = (bf16[2,3072]{1,0:T(2,128)(2,1)S(1)}, bf16[2,3072]{1,0:T(2,128)(2,1)S(1)}, u32[]{:S(2)}, u32[]{:S(2)}) collective-permute-start(bf16[2,3072]{1,0:T(2,128)(2,1)S(1)} %get-tuple-element.7), channel_id=1, source_target_pairs={{2,0},{4,2},{6,4},{8,6},{10,8},{12,10},{14,12},{3,1},{5,3},{7,5},{... | collective-permute-start | bytes 36872 | tf_op jit(solution)/shard_map/ppermute | solution.py:31
  69.8 6.3 %copy-start.3 = (bf16[1,8,128]{2,1,0:T(8,128)(2,1)S(1)}, bf16[1,8,128]{2,1,0:T(8,128)(2,1)}, u32[]{:S(2)}) copy-start(bf16[1,8,128]{2,1,0:T(8,128)(2,1)} %param.20) | copy-start | bytes 6148
  69.8 72.0 %all-to-all-start = ((bf16[8,2,2,32,1024]{4,3,2,1,0:T(8,128)(2,1)}), bf16[8,2,2,32,1024]{4,3,2,1,0:T(8,128)(2,1)S(1)}, u32[]{:S(2)}, u32[]{:S(2)}) async-start(bf16[8,2,2,32,1024]{4,3,2,1,0:T(8,128)(2,1)} %fusion.10), calls=%async_computation | async-start | bytes 4194304 | tf_op jit(solution)/shard_map/all_to_all | solution.py:18
  75.4 102.2 %copy-start.1 = (bf16[1,32,64]{2,1,0:T(8,128)(2,1)S(1)}, bf16[1,32,64]{2,1,0:T(8,128)(2,1)}, u32[]{:S(2)}) copy-start(bf16[1,32,64]{2,1,0:T(8,128)(2,1)} %param.21) | copy-start | bytes 12292
  75.5 106.6 %copy-start.2 = (f32[32,64]{1,0:T(8,128)S(1)}, f32[32,64]{1,0:T(8,128)}, u32[]{:S(2)}) copy-start(f32[32,64]{1,0:T(8,128)} %param.23) | copy-start | bytes 24580
Sparse Core Ops, SparseCore 0:
  9.5 11.7 all-gather.2
